TPU v7x, 32 devices: a whole 2x2x4 slice. The times are simulated.
32 devices in a mesh: fs: 16 (over z, y, x), tp: 2 (over core).
Axes of the slice: x: 2, y: 2, z: 4, core: 2. Of those that a mesh axis runs over, the one named last changes fastest.
Arguments:
- saved_inputs: bfloat16 [12288, 2048], P('fs'), may hold values from -6 to 6
- cotangents: bfloat16 [3, 12288, 1024], P(None, 'fs', 'tp'), may hold values from -0.0546875 to 0.0546875
- left_roots: float32 [3, 2048, 2048], P(None, 'fs'), may hold values from -1 to 2
- right_roots: float32 [3, 1024, 128], P(None, 'tp'), may hold values from -1 to 2
- moments: float32 [3, 2048, 1024], P(None, 'fs', 'tp'), may hold values from -125 to 125
- masters: float32 [3, 2048, 1024], P(None, 'fs', 'tp'), may hold values from -3 to 3
Outputs:
- direction: float32 [3, 2048, 1024], P(None, 'fs', 'tp')
- moments_new: float32 [3, 2048, 1024], P(None, 'fs', 'tp')
- copies: bfloat16 [3, 2048, 1024], P(None, None, 'tp')
All inputs are finite; a program needn't handle non-finite values.
Results may differ from a plain program's by a relative error of at most 0.002.
Values may be sent and summed in bfloat16 or wider, within the bound.
A program may use at most 64 MiB of HBM per device.

v0:
```python
import jax
import jax.numpy as jnp
from jax import lax
from jax.sharding import PartitionSpec as P

D = 2048
SBW = 1024
RB = 128
momentum_decay = 0.9
step_rate = 0.1
eps_value = 1e-06


def on_device(saved_inputs, cotangents, left_roots, right_roots, moments, masters):
    rows_own = masters.shape[1]
    columns = masters.shape[2]
    grad_rows = lax.psum_scatter(
        jnp.einsum("td,mtc->dmc", saved_inputs, cotangents, preferred_element_type=jnp.float32),
        "fs",
        scatter_dimension=0,
        tiled=True,
    )
    empty = jnp.zeros((3, rows_own, columns), jnp.float32)
    left_done = empty + jnp.einsum(
        "mrn,nmc->mrc",
        left_roots,
        lax.all_gather(grad_rows.astype(jnp.bfloat16), "fs", axis=0, tiled=True).astype(
            jnp.float32
        ),
        precision=lax.Precision.HIGHEST,
    )
    block_count = columns // RB
    right_blocks = right_roots.reshape(3, block_count, RB, RB)
    right_done = jnp.einsum(
        "mrbi,mbij->mrbj",
        left_done.reshape(3, rows_own, block_count, RB),
        right_blocks,
        precision=lax.Precision.HIGHEST,
    ).reshape(3, rows_own, columns)
    moments_new = momentum_decay * moments + right_done
    totals = lax.psum(jnp.sum(moments_new * moments_new, axis=(1, 2)), ("fs", "tp"))
    meansq = totals / (D * SBW)
    direction = moments_new * lax.rsqrt(meansq + eps_value)[:, None, None]
    copy_rows = (masters - step_rate * direction).astype(jnp.bfloat16)
    copies = lax.all_gather(copy_rows, "fs", axis=1, tiled=True)
    return (direction, moments_new, copies)


def solution(mesh):
    placed = (
        P("fs", None),
        P(None, "fs", "tp"),
        P(None, "fs", None),
        P(None, "tp", None),
        P(None, "fs", "tp"),
        P(None, "fs", "tp"),
    )
    return jax.shard_map(
        on_device,
        mesh=mesh,
        in_specs=placed,
        out_specs=(P(None, "fs", "tp"), P(None, "fs", "tp"), P(None, None, "tp")),
        check_vma=False,
    )
```

profile of v0, /device:TPU:0, one launch (start us, length us, event | category | flops | bytes accessed | tf_op | source)
XLA Modules:
  0.0 505.3 jit_solution(11344276064925415366)
XLA Ops:
  7.2 0.0 copy-start
  7.2 0.0 reduce-scatter.2.cloned.1.call-start
  7.2 1.8 copy-done
  9.1 9.7 %fusion = f32[2048,3,512]{0,2,1:T(8,128)} fusion(bf16[3,768,512]{2,1,0:T(8,128)(2,1)} %param.7, bf16[768,2048]{1,0:T(8,128)(2,1)S(1)} %copy-done), kind=kOutput, calls=%fused_computation | convolution fusion | flops 4831838208 | bytes 18087936 | tf_op jit(solution)/shard_map/td,mtc->dmc/dot_general | solution.py:18
  18.7 0.0 reduce-scatter.2.cloned.1.call-update
  18.7 0.0 all-gather.3.cloned.1.call-start
  18.8 205.6 %reduce-scatter.2.cloned.1.call-done = f32[128,3,512]{0,2,1:T(8,128)} async-done(((f32[2048,3,512]{0,2,1:T(8,128)}), f32[128,3,512]{0,2,1:T(8,128)}) %reduce-scatter.2.cloned.1.call-update) | async-done | bytes 786448 | tf_op jit(solution)/shard_map/reduce_scatter | solution.py:17
  224.4 1.9 convert_element_type.7
  226.3 0.0 all-gather.3.cloned.1.call-update
  226.3 0.0 all-gather.5.cloned.1.call-start
  226.4 115.8 %all-gather.3.cloned.1.call-done = bf16[2048,3,512]{0,2,1:T(8,128)(2,1)} async-done(((bf16[128,3,512]{0,2,1:T(8,128)(2,1)}), bf16[2048,3,512]{0,2,1:T(8,128)(2,1)}) %all-gather.3.cloned.1.call-update) | async-done | bytes 6291472 | tf_op jit(solution)/shard_map/all_gather | solution.py:27
  342.2 0.0 copy-start.1
  342.2 8.4 %fusion.2 = f32[3,512,128]{2,1,0:T(8,128)S(1)} fusion(bf16[2048,3,512]{0,2,1:T(8,128)(2,1)} %all-gather.3.cloned.1.call-done, f32[3,128,2048]{2,1,0:T(8,128)} %param.8), kind=kOutput, calls=%fused_computation.7 | convolution fusion | flops 4831838208 | bytes 10223616 | tf_op jit(solution)/shard_map/mrn,nmc->mrc/dot_general | solution.py:24
  350.6 0.0 copy-done.1
  350.6 2.3 fusion.3
  352.9 2.3 copy.11
  355.2 2.4 multiply_reduce_fusion
  357.6 38.3 %psum.7 = f32[3]{0:T(128)S(1)} all-reduce(f32[3]{0:T(128)S(1)} %get-tuple-element.5), channel_id=1, replica_groups=mesh['fs'=16,'tp'=2] {'fs','tp'}, use_global_device_ids=true, to_apply=%region_2.0 | all-reduce | flops 3 | bytes 24 | tf_op jit(solution)/shard_map/psum | solution.py:41
  395.9 2.6 subtract_convert_fusion
  398.5 0.0 all-gather.5.cloned.1.call-update
  398.6 94.3 %all-gather.5.cloned.1.call-done = bf16[3,2048,512]{2,1,0:T(8,128)(2,1)} async-done(((bf16[3,128,512]{2,1,0:T(8,128)(2,1)}), bf16[3,2048,512]{2,1,0:T(8,128)(2,1)}) %all-gather.5.cloned.1.call-update) | async-done | bytes 6291472 | tf_op jit(solution)/shard_map/all_gather | solution.py:45
  492.9 5.9 %copy.15 = bf16[3,2048,512]{2,1,0:T(8,128)(2,1)} copy(bf16[3,2048,512]{2,1,0:T(8,128)(2,1)} %all-gather.5.cloned.1.call-done) | data formatting | bytes 12582912
  (1 shorter events, 0.0 us)
Async XLA Ops:
  7.2 1.9 copy-start
  7.2 217.2 %reduce-scatter.2.cloned.1.call-start = ((), (), s32[]{:S(2)}) async-start(), calls=%async_computation.1 | async-start | bytes 13369344 | tf_op jit(solution)/shard_map/reduce_scatter | solution.py:17
  18.7 323.4 %all-gather.3.cloned.1.call-start = ((), (), s32[]{:S(2)}) async-start(), calls=%async_computation.2 | async-start | bytes 6684672 | tf_op jit(solution)/shard_map/all_gather | solution.py:27
  226.3 266.5 %all-gather.5.cloned.1.call-start = ((), (), s32[]{:S(2)}) async-start(), calls=%async_computation.3 | async-start | bytes 6684672 | tf_op jit(solution)/shard_map/all_gather | solution.py:45
  342.2 8.4 %copy-start.1 = (f32[3,512,128]{2,1,0:T(8,128)S(1)}, f32[3,512,128]{2,1,0:T(8,128)}, u32[]{:S(2)}) copy-start(f32[3,512,128]{2,1,0:T(8,128)} %param.9) | copy-start | bytes 2359300
Sparse Core Ops, SparseCore 0:
  18.9 205.4 reduce-scatter.1
  227.7 114.4 all-gather.2
  398.7 94.1 all-gather.4
where the time goes:
time: 506 us; the launch traced here: 505 us
  waiting for transfers between devices  416 us (82%)
  blocking collectives  38.3 us (8%)
  matrix products  20.4 us (4%)
  between operations  13.8 us (3%)
  local copies, waits for them, and re-layouts  10 us (2%)
  other arithmetic  6.93 us (1%)
    reduce_scatter x1, waiting for transfers between devices, on_device(): lax.psum_scatter(jnp.einsum('td,mtc->dmc', saved_inputs, cotangents, pref...  206 us
    all_gather x1, waiting for transfers between devices, on_device(): lax.all_gather(grad_rows.astype(jnp.bfloat16), 'fs', axis=0, tiled=True)  116 us
    all_gather x1, waiting for transfers between devices, on_device(): copies = lax.all_gather(copy_rows, 'fs', axis=1, tiled=True)  94.3 us
    psum x1, blocking collectives, on_device(): lax.psum(jnp.sum(moments_new * moments_new, axis=(1, 2)), ('fs', 'tp'))  38.3 us
  transfers between devices with their start and end apart: 3, of which 3 were waited for; matrix products, arithmetic and copies ran while one was open for 0% of the time, Pallas kernels for 0%

commit v1 on v0

--- a/solution.py
+++ b/solution.py
@@ -9,6 +9,17 @@
 momentum_decay = 0.9
 step_rate = 0.1
 eps_value = 1e-06
+
+
+def gather_by_hops(shard, axis, along):
+    devices = lax.axis_size(axis)
+    forward = [(i, (i + 1) % devices) for i in range(devices)]
+    parts = [shard]
+    for far in range(1, devices):
+        parts = [lax.ppermute(parts[0], axis, forward), *parts]
+    whole = jnp.concatenate(parts, axis=along)
+    offset = (lax.axis_index(axis) + 1) * parts[-1].shape[along]
+    return jnp.roll(whole, offset, axis=along)
 
 
 def on_device(saved_inputs, cotangents, left_roots, right_roots, moments, masters):
@@ -42,7 +53,7 @@
     meansq = totals / (D * SBW)
     direction = moments_new * lax.rsqrt(meansq + eps_value)[:, None, None]
     copy_rows = (masters - step_rate * direction).astype(jnp.bfloat16)
-    copies = lax.all_gather(copy_rows, "fs", axis=1, tiled=True)
+    copies = gather_by_hops(copy_rows, "fs", 1)
     return (direction, moments_new, copies)
 
 

time: 506 us -> 630 us (1.25)
  waiting for transfers between devices: 416 us -> 511 us
  local copies, waits for them, and re-layouts: 10 us -> 34.9 us
    ppermute x0 -> x15, waiting for transfers between devices: none -> 190 us  [gather_by_hops(): parts = [lax.ppermute(parts[0], axis, forward), *parts]]
    all_gather x1 -> x0, waiting for transfers between devices: 94.3 us -> none  [on_device(): copies = lax.all_gather(copy_rows, 'fs', axis=1, tiled=True)]
    unnamed x5 -> x87, local copies, waits for them, and re-layouts: 7.74 us -> 29.5 us
  transfers between devices with their start and end apart: 3 -> 17, of which waited for: 3 -> 17; matrix products, arithmetic and copies ran while one was open for 0% -> 0% of each run, Pallas kernels for 0% -> 0%
where the time goes in v1:
time: 630 us; the launch traced here: 629 us
  waiting for transfers between devices  511 us (81%)
  blocking collectives  38.3 us (6%)
  local copies, waits for them, and re-layouts  34.9 us (6%)
  matrix products  20.4 us (3%)
  between operations  14.5 us (2%)
  other arithmetic  6.81 us (1%)
    reduce_scatter x1, waiting for transfers between devices, on_device(): lax.psum_scatter(jnp.einsum('td,mtc->dmc', saved_inputs, cotangents, pref...  206 us
    ppermute x15, waiting for transfers between devices, gather_by_hops(): parts = [lax.ppermute(parts[0], axis, forward), *parts]  190 us
    all_gather x1, waiting for transfers between devices, on_device(): lax.all_gather(grad_rows.astype(jnp.bfloat16), 'fs', axis=0, tiled=True)  116 us
    psum x1, blocking collectives, on_device(): lax.psum(jnp.sum(moments_new * moments_new, axis=(1, 2)), ('fs', 'tp'))  38.3 us
    unnamed x87, local copies, waits for them, and re-layouts  29.5 us
  transfers between devices with their start and end apart: 17, of which 17 were waited for; matrix products, arithmetic and copies ran while one was open for 0% of the time, Pallas kernels for 0%

profile of v1, /device:TPU:0, one launch (start us, length us, event | category | flops | bytes accessed | tf_op | source)
XLA Modules:
  0.0 628.6 jit_solution(2265179701594666167)
XLA Ops:
  7.2 1.8 copy-done
  9.1 9.7 %fusion = f32[2048,3,512]{0,2,1:T(8,128)} fusion(bf16[3,768,512]{2,1,0:T(8,128)(2,1)} %param.7, bf16[768,2048]{1,0:T(8,128)(2,1)S(1)} %copy-done), kind=kOutput, calls=%fused_computation | convolution fusion | flops 4831838208 | bytes 18087936 | tf_op jit(solution)/shard_map/td,mtc->dmc/dot_general | solution.py:29
  18.8 205.6 %reduce-scatter.2.cloned.1.call-done = f32[128,3,512]{0,2,1:T(8,128)} async-done(((f32[2048,3,512]{0,2,1:T(8,128)}), f32[128,3,512]{0,2,1:T(8,128)}) %reduce-scatter.2.cloned.1.call-update) | async-done | bytes 786448 | tf_op jit(solution)/shard_map/reduce_scatter | solution.py:28
  224.4 1.9 convert_element_type.7
  226.3 115.8 %all-gather.2.cloned.1.call-done = bf16[2048,3,512]{0,2,1:T(8,128)(2,1)} async-done(((bf16[128,3,512]{0,2,1:T(8,128)(2,1)}), bf16[2048,3,512]{0,2,1:T(8,128)(2,1)}) %all-gather.2.cloned.1.call-update) | async-done | bytes 6291472 | tf_op jit(solution)/shard_map/all_gather | solution.py:38
  342.2 8.4 %fusion.2 = f32[3,512,128]{2,1,0:T(8,128)S(1)} fusion(bf16[2048,3,512]{0,2,1:T(8,128)(2,1)} %all-gather.2.cloned.1.call-done, f32[3,128,2048]{2,1,0:T(8,128)} %param.8), kind=kOutput, calls=%fused_computation.40 | convolution fusion | flops 4831838208 | bytes 10223616 | tf_op jit(solution)/shard_map/mrn,nmc->mrc/dot_general | solution.py:35
  350.6 2.3 fusion.3
  352.9 2.3 copy.11
  355.2 2.4 multiply_reduce_fusion
  357.6 38.3 %psum.7 = f32[3]{0:T(128)S(1)} all-reduce(f32[3]{0:T(128)S(1)} %get-tuple-element.5), channel_id=1, replica_groups=mesh['fs'=16,'tp'=2] {'fs','tp'}, use_global_device_ids=true, to_apply=%region_2.0 | all-reduce | flops 3 | bytes 24 | tf_op jit(solution)/shard_map/psum | solution.py:52
  395.9 2.5 subtract_convert_fusion
  398.4 2.3 collective-permute-start
  400.7 11.4 %collective-permute-done = bf16[3,128,512]{2,1,0:T(8,128)(2,1)S(1)} collective-permute-done((bf16[3,128,512]{2,1,0:T(8,128)(2,1)S(1)}, bf16[3,128,512]{2,1,0:T(8,128)(2,1)S(1)}, u32[]{:S(2)}, u32[]{:S(2)}) %collective-permute-start) | collective-permute-done | bytes 393248 | tf_op jit(solution)/shard_map/ppermute | solution.py:19
  412.8 12.8 %collective-permute-done.1 = bf16[3,128,512]{2,1,0:T(8,128)(2,1)S(1)} collective-permute-done((bf16[3,128,512]{2,1,0:T(8,128)(2,1)S(1)}, bf16[3,128,512]{2,1,0:T(8,128)(2,1)S(1)}, u32[]{:S(2)}, u32[]{:S(2)}) %collective-permute-start.1) | collective-permute-done | bytes 393248 | tf_op jit(solution)/shard_map/ppermute | solution.py:19
  426.3 11.9 %collective-permute-done.2 = bf16[3,128,512]{2,1,0:T(8,128)(2,1)S(1)} collective-permute-done((bf16[3,128,512]{2,1,0:T(8,128)(2,1)S(1)}, bf16[3,128,512]{2,1,0:T(8,128)(2,1)S(1)}, u32[]{:S(2)}, u32[]{:S(2)}) %collective-permute-start.2) | collective-permute-done | bytes 393248 | tf_op jit(solution)/shard_map/ppermute | solution.py:19
  439.0 11.4 %collective-permute-done.3 = bf16[3,128,512]{2,1,0:T(8,128)(2,1)S(1)} collective-permute-done((bf16[3,128,512]{2,1,0:T(8,128)(2,1)S(1)}, bf16[3,128,512]{2,1,0:T(8,128)(2,1)S(1)}, u32[]{:S(2)}, u32[]{:S(2)}) %collective-permute-start.3) | collective-permute-done | bytes 393248 | tf_op jit(solution)/shard_map/ppermute | solution.py:19
  451.2 11.4 %collective-permute-done.4 = bf16[3,128,512]{2,1,0:T(8,128)(2,1)S(1)} collective-permute-done((bf16[3,128,512]{2,1,0:T(8,128)(2,1)S(1)}, bf16[3,128,512]{2,1,0:T(8,128)(2,1)S(1)}, u32[]{:S(2)}, u32[]{:S(2)}) %collective-permute-start.4) | collective-permute-done | bytes 393248 | tf_op jit(solution)/shard_map/ppermute | solution.py:19
  463.3 11.4 %collective-permute-done.5 = bf16[3,128,512]{2,1,0:T(8,128)(2,1)S(1)} collective-permute-done((bf16[3,128,512]{2,1,0:T(8,128)(2,1)S(1)}, bf16[3,128,512]{2,1,0:T(8,128)(2,1)S(1)}, u32[]{:S(2)}, u32[]{:S(2)}) %collective-permute-start.5) | collective-permute-done | bytes 393248 | tf_op jit(solution)/shard_map/ppermute | solution.py:19
  475.5 12.6 %collective-permute-done.6 = bf16[3,128,512]{2,1,0:T(8,128)(2,1)S(1)} collective-permute-done((bf16[3,128,512]{2,1,0:T(8,128)(2,1)S(1)}, bf16[3,128,512]{2,1,0:T(8,128)(2,1)S(1)}, u32[]{:S(2)}, u32[]{:S(2)}) %collective-permute-start.6) | collective-permute-done | bytes 393248 | tf_op jit(solution)/shard_map/ppermute | solution.py:19
  488.8 13.7 %collective-permute-done.7 = bf16[3,128,512]{2,1,0:T(8,128)(2,1)S(1)} collective-permute-done((bf16[3,128,512]{2,1,0:T(8,128)(2,1)S(1)}, bf16[3,128,512]{2,1,0:T(8,128)(2,1)S(1)}, u32[]{:S(2)}, u32[]{:S(2)}) %collective-permute-start.7) | collective-permute-done | bytes 393248 | tf_op jit(solution)/shard_map/ppermute | solution.py:19
  503.2 14.9 %collective-permute-done.8 = bf16[3,128,512]{2,1,0:T(8,128)(2,1)S(1)} collective-permute-done((bf16[3,128,512]{2,1,0:T(8,128)(2,1)S(1)}, bf16[3,128,512]{2,1,0:T(8,128)(2,1)S(1)}, u32[]{:S(2)}, u32[]{:S(2)}) %collective-permute-start.8) | collective-permute-done | bytes 393248 | tf_op jit(solution)/shard_map/ppermute | solution.py:19
  518.9 15.1 %collective-permute-done.9 = bf16[3,128,512]{2,1,0:T(8,128)(2,1)S(1)} collective-permute-done((bf16[3,128,512]{2,1,0:T(8,128)(2,1)S(1)}, bf16[3,128,512]{2,1,0:T(8,128)(2,1)S(1)}, u32[]{:S(2)}, u32[]{:S(2)}) %collective-permute-start.9) | collective-permute-done | bytes 393248 | tf_op jit(solution)/shard_map/ppermute | solution.py:19
  534.7 14.3 %collective-permute-done.10 = bf16[3,128,512]{2,1,0:T(8,128)(2,1)S(1)} collective-permute-done((bf16[3,128,512]{2,1,0:T(8,128)(2,1)S(1)}, bf16[3,128,512]{2,1,0:T(8,128)(2,1)S(1)}, u32[]{:S(2)}, u32[]{:S(2)}) %collective-permute-start.10) | collective-permute-done | bytes 393248 | tf_op jit(solution)/shard_map/ppermute | solution.py:19
  549.8 13.4 %collective-permute-done.11 = bf16[3,128,512]{2,1,0:T(8,128)(2,1)S(1)} collective-permute-done((bf16[3,128,512]{2,1,0:T(8,128)(2,1)S(1)}, bf16[3,128,512]{2,1,0:T(8,128)(2,1)S(1)}, u32[]{:S(2)}, u32[]{:S(2)}) %collective-permute-start.11) | collective-permute-done | bytes 393248 | tf_op jit(solution)/shard_map/ppermute | solution.py:19
  564.0 12.6 %collective-permute-done.12 = bf16[3,128,512]{2,1,0:T(8,128)(2,1)S(1)} collective-permute-done((bf16[3,128,512]{2,1,0:T(8,128)(2,1)S(1)}, bf16[3,128,512]{2,1,0:T(8,128)(2,1)S(1)}, u32[]{:S(2)}, u32[]{:S(2)}) %collective-permute-start.12) | collective-permute-done | bytes 393248 | tf_op jit(solution)/shard_map/ppermute | solution.py:19
  577.3 11.5 %collective-permute-done.13 = bf16[3,128,512]{2,1,0:T(8,128)(2,1)} collective-permute-done((bf16[3,128,512]{2,1,0:T(8,128)(2,1)S(1)}, bf16[3,128,512]{2,1,0:T(8,128)(2,1)}, u32[]{:S(2)}, u32[]{:S(2)}) %collective-permute-start.13) | collective-permute-done | bytes 393248 | tf_op jit(solution)/shard_map/ppermute | solution.py:19
  588.9 11.6 %collective-permute-done.14 = bf16[3,128,512]{2,1,0:T(8,128)(2,1)} collective-permute-done((bf16[3,128,512]{2,1,0:T(8,128)(2,1)}, bf16[3,128,512]{2,1,0:T(8,128)(2,1)}, u32[]{:S(2)}, u32[]{:S(2)}) %collective-permute-start.14) | collective-permute-done | bytes 393248 | tf_op jit(solution)/shard_map/ppermute | solution.py:19
  601.5 1.0 constant_dynamic-update-slice_fusion.30
  602.6 1.0 constant_dynamic-update-slice_fusion.29
  603.6 1.0 constant_dynamic-update-slice_fusion.28
  604.6 1.0 constant_dynamic-update-slice_fusion.27
  618.6 3.1 constant_dynamic-slice_fusion
  (102 shorter events, 23.7 us)
Async XLA Ops:
  7.2 1.9 copy-start
  7.2 217.2 %reduce-scatter.2.cloned.1.call-start = ((), (), s32[]{:S(2)}) async-start(), calls=%async_computation.1 | async-start | bytes 13369344 | tf_op jit(solution)/shard_map/reduce_scatter | solution.py:28
  18.7 323.4 %all-gather.2.cloned.1.call-start = ((), (), s32[]{:S(2)}) async-start(), calls=%async_computation.2 | async-start | bytes 6684672 | tf_op jit(solution)/shard_map/all_gather | solution.py:38
  342.2 8.4 %copy-start.27 = (f32[3,512,128]{2,1,0:T(8,128)S(1)}, f32[3,512,128]{2,1,0:T(8,128)}, u32[]{:S(2)}) copy-start(f32[3,512,128]{2,1,0:T(8,128)} %param.9) | copy-start | bytes 2359300
  398.4 13.6 %collective-permute-start = (bf16[3,128,512]{2,1,0:T(8,128)(2,1)S(1)}, bf16[3,128,512]{2,1,0:T(8,128)(2,1)S(1)}, u32[]{:S(2)}, u32[]{:S(2)}) collective-permute-start(bf16[3,128,512]{2,1,0:T(8,128)(2,1)S(1)} %get-tuple-element.3), channel_id=1, source_target_pairs={{0,2},{2,4},{4,6},{6,8},{8,10},{10,12},{12,14},{14,16},{16,18},{18... | collective-permute-start | bytes 1179656 | tf_op jit(solution)/shard_map/ppermute | solution.py:19
  412.8 12.8 %collective-permute-start.1 = (bf16[3,128,512]{2,1,0:T(8,128)(2,1)S(1)}, bf16[3,128,512]{2,1,0:T(8,128)(2,1)S(1)}, u32[]{:S(2)}, u32[]{:S(2)}) collective-permute-start(bf16[3,128,512]{2,1,0:T(8,128)(2,1)S(1)} %collective-permute-done), channel_id=1, source_target_pairs={{0,2},{2,4},{4,6},{6,8},{8,10},{10,12},{12,14},{14,16},{16,18},{18... | collective-permute-start | bytes 1179656 | tf_op jit(solution)/shard_map/ppermute | solution.py:19
  426.3 11.9 %collective-permute-start.2 = (bf16[3,128,512]{2,1,0:T(8,128)(2,1)S(1)}, bf16[3,128,512]{2,1,0:T(8,128)(2,1)S(1)}, u32[]{:S(2)}, u32[]{:S(2)}) collective-permute-start(bf16[3,128,512]{2,1,0:T(8,128)(2,1)S(1)} %collective-permute-done.1), channel_id=1, source_target_pairs={{0,2},{2,4},{4,6},{6,8},{8,10},{10,12},{12,14},{14,16},{16,18},{18... | collective-permute-start | bytes 1179656 | tf_op jit(solution)/shard_map/ppermute | solution.py:19
  439.0 11.4 %collective-permute-start.3 = (bf16[3,128,512]{2,1,0:T(8,128)(2,1)S(1)}, bf16[3,128,512]{2,1,0:T(8,128)(2,1)S(1)}, u32[]{:S(2)}, u32[]{:S(2)}) collective-permute-start(bf16[3,128,512]{2,1,0:T(8,128)(2,1)S(1)} %collective-permute-done.2), channel_id=1, source_target_pairs={{0,2},{2,4},{4,6},{6,8},{8,10},{10,12},{12,14},{14,16},{16,18},{18... | collective-permute-start | bytes 1179656 | tf_op jit(solution)/shard_map/ppermute | solution.py:19
  451.2 11.4 %collective-permute-start.4 = (bf16[3,128,512]{2,1,0:T(8,128)(2,1)S(1)}, bf16[3,128,512]{2,1,0:T(8,128)(2,1)S(1)}, u32[]{:S(2)}, u32[]{:S(2)}) collective-permute-start(bf16[3,128,512]{2,1,0:T(8,128)(2,1)S(1)} %collective-permute-done.3), channel_id=1, source_target_pairs={{0,2},{2,4},{4,6},{6,8},{8,10},{10,12},{12,14},{14,16},{16,18},{18... | collective-permute-start | bytes 1179656 | tf_op jit(solution)/shard_map/ppermute | solution.py:19
  463.3 11.4 %collective-permute-start.5 = (bf16[3,128,512]{2,1,0:T(8,128)(2,1)S(1)}, bf16[3,128,512]{2,1,0:T(8,128)(2,1)S(1)}, u32[]{:S(2)}, u32[]{:S(2)}) collective-permute-start(bf16[3,128,512]{2,1,0:T(8,128)(2,1)S(1)} %collective-permute-done.4), channel_id=1, source_target_pairs={{0,2},{2,4},{4,6},{6,8},{8,10},{10,12},{12,14},{14,16},{16,18},{18... | collective-permute-start | bytes 1179656 | tf_op jit(solution)/shard_map/ppermute | solution.py:19
  475.5 12.6 %collective-permute-start.6 = (bf16[3,128,512]{2,1,0:T(8,128)(2,1)S(1)}, bf16[3,128,512]{2,1,0:T(8,128)(2,1)S(1)}, u32[]{:S(2)}, u32[]{:S(2)}) collective-permute-start(bf16[3,128,512]{2,1,0:T(8,128)(2,1)S(1)} %collective-permute-done.5), channel_id=1, source_target_pairs={{0,2},{2,4},{4,6},{6,8},{8,10},{10,12},{12,14},{14,16},{16,18},{18... | collective-permute-start | bytes 1179656 | tf_op jit(solution)/shard_map/ppermute | solution.py:19
  488.8 13.7 %collective-permute-start.7 = (bf16[3,128,512]{2,1,0:T(8,128)(2,1)S(1)}, bf16[3,128,512]{2,1,0:T(8,128)(2,1)S(1)}, u32[]{:S(2)}, u32[]{:S(2)}) collective-permute-start(bf16[3,128,512]{2,1,0:T(8,128)(2,1)S(1)} %collective-permute-done.6), channel_id=1, source_target_pairs={{0,2},{2,4},{4,6},{6,8},{8,10},{10,12},{12,14},{14,16},{16,18},{18... | collective-permute-start | bytes 1179656 | tf_op jit(solution)/shard_map/ppermute | solution.py:19
  503.2 14.9 %collective-permute-start.8 = (bf16[3,128,512]{2,1,0:T(8,128)(2,1)S(1)}, bf16[3,128,512]{2,1,0:T(8,128)(2,1)S(1)}, u32[]{:S(2)}, u32[]{:S(2)}) collective-permute-start(bf16[3,128,512]{2,1,0:T(8,128)(2,1)S(1)} %collective-permute-done.7), channel_id=1, source_target_pairs={{0,2},{2,4},{4,6},{6,8},{8,10},{10,12},{12,14},{14,16},{16,18},{18... | collective-permute-start | bytes 1179656 | tf_op jit(solution)/shard_map/ppermute | solution.py:19
  518.8 15.1 %collective-permute-start.9 = (bf16[3,128,512]{2,1,0:T(8,128)(2,1)S(1)}, bf16[3,128,512]{2,1,0:T(8,128)(2,1)S(1)}, u32[]{:S(2)}, u32[]{:S(2)}) collective-permute-start(bf16[3,128,512]{2,1,0:T(8,128)(2,1)S(1)} %collective-permute-done.8), channel_id=1, source_target_pairs={{0,2},{2,4},{4,6},{6,8},{8,10},{10,12},{12,14},{14,16},{16,18},{18... | collective-permute-start | bytes 1179656 | tf_op jit(solution)/shard_map/ppermute | solution.py:19
  534.7 14.3 %collective-permute-start.10 = (bf16[3,128,512]{2,1,0:T(8,128)(2,1)S(1)}, bf16[3,128,512]{2,1,0:T(8,128)(2,1)S(1)}, u32[]{:S(2)}, u32[]{:S(2)}) collective-permute-start(bf16[3,128,512]{2,1,0:T(8,128)(2,1)S(1)} %collective-permute-done.9), channel_id=1, source_target_pairs={{0,2},{2,4},{4,6},{6,8},{8,10},{10,12},{12,14},{14,16},{16,18},{18... | collective-permute-start | bytes 1179656 | tf_op jit(solution)/shard_map/ppermute | solution.py:19
  549.8 13.5 %collective-permute-start.11 = (bf16[3,128,512]{2,1,0:T(8,128)(2,1)S(1)}, bf16[3,128,512]{2,1,0:T(8,128)(2,1)S(1)}, u32[]{:S(2)}, u32[]{:S(2)}) collective-permute-start(bf16[3,128,512]{2,1,0:T(8,128)(2,1)S(1)} %collective-permute-done.10), channel_id=1, source_target_pairs={{0,2},{2,4},{4,6},{6,8},{8,10},{10,12},{12,14},{14,16},{16,18},{18... | collective-permute-start | bytes 1179656 | tf_op jit(solution)/shard_map/ppermute | solution.py:19
  564.0 12.6 %collective-permute-start.12 = (bf16[3,128,512]{2,1,0:T(8,128)(2,1)S(1)}, bf16[3,128,512]{2,1,0:T(8,128)(2,1)S(1)}, u32[]{:S(2)}, u32[]{:S(2)}) collective-permute-start(bf16[3,128,512]{2,1,0:T(8,128)(2,1)S(1)} %collective-permute-done.11), channel_id=1, source_target_pairs={{0,2},{2,4},{4,6},{6,8},{8,10},{10,12},{12,14},{14,16},{16,18},{18... | collective-permute-start | bytes 1179656 | tf_op jit(solution)/shard_map/ppermute | solution.py:19
  577.3 11.5 %collective-permute-start.13 = (bf16[3,128,512]{2,1,0:T(8,128)(2,1)S(1)}, bf16[3,128,512]{2,1,0:T(8,128)(2,1)}, u32[]{:S(2)}, u32[]{:S(2)}) collective-permute-start(bf16[3,128,512]{2,1,0:T(8,128)(2,1)S(1)} %collective-permute-done.12), channel_id=1, source_target_pairs={{0,2},{2,4},{4,6},{6,8},{8,10},{10,12},{12,14},{14,16},{16,18},{18... | collective-permute-start | bytes 1179656 | tf_op jit(solution)/shard_map/ppermute | solution.py:19
  588.8 11.7 %collective-permute-start.14 = (bf16[3,128,512]{2,1,0:T(8,128)(2,1)}, bf16[3,128,512]{2,1,0:T(8,128)(2,1)}, u32[]{:S(2)}, u32[]{:S(2)}) collective-permute-start(bf16[3,128,512]{2,1,0:T(8,128)(2,1)} %collective-permute-done.13), channel_id=1, source_target_pairs={{0,2},{2,4},{4,6},{6,8},{8,10},{10,12},{12,14},{14,16},{16,18},{18... | collective-permute-start | bytes 1179656 | tf_op jit(solution)/shard_map/ppermute | solution.py:19
  588.8 29.2 %copy-start.26 = (bf16[3,128,512]{2,1,0:T(8,128)(2,1)S(1)}, bf16[3,128,512]{2,1,0:T(8,128)(2,1)}, u32[]{:S(2)}) copy-start(bf16[3,128,512]{2,1,0:T(8,128)(2,1)} %copy-done.25) | copy-start | bytes 1179652
  588.8 29.2 %copy-start.24 = (bf16[3,128,512]{2,1,0:T(8,128)(2,1)S(1)}, bf16[3,128,512]{2,1,0:T(8,128)(2,1)}, u32[]{:S(2)}) copy-start(bf16[3,128,512]{2,1,0:T(8,128)(2,1)} %copy-done.23) | copy-start | bytes 1179652
  588.8 29.3 %copy-start.22 = (bf16[3,128,512]{2,1,0:T(8,128)(2,1)S(1)}, bf16[3,128,512]{2,1,0:T(8,128)(2,1)}, u32[]{:S(2)}) copy-start(bf16[3,128,512]{2,1,0:T(8,128)(2,1)} %copy-done.21) | copy-start | bytes 1179652
  588.8 29.3 %copy-start.20 = (bf16[3,128,512]{2,1,0:T(8,128)(2,1)S(1)}, bf16[3,128,512]{2,1,0:T(8,128)(2,1)}, u32[]{:S(2)}) copy-start(bf16[3,128,512]{2,1,0:T(8,128)(2,1)} %copy-done.19) | copy-start | bytes 1179652
  588.8 29.3 %copy-start.18 = (bf16[3,128,512]{2,1,0:T(8,128)(2,1)S(1)}, bf16[3,128,512]{2,1,0:T(8,128)(2,1)}, u32[]{:S(2)}) copy-start(bf16[3,128,512]{2,1,0:T(8,128)(2,1)} %copy-done.17) | copy-start | bytes 1179652
  588.8 29.4 %copy-start.16 = (bf16[3,128,512]{2,1,0:T(8,128)(2,1)S(1)}, bf16[3,128,512]{2,1,0:T(8,128)(2,1)}, u32[]{:S(2)}) copy-start(bf16[3,128,512]{2,1,0:T(8,128)(2,1)} %copy-done.15) | copy-start | bytes 1179652
  588.9 29.4 %copy-start.14 = (bf16[3,128,512]{2,1,0:T(8,128)(2,1)S(1)}, bf16[3,128,512]{2,1,0:T(8,128)(2,1)}, u32[]{:S(2)}) copy-start(bf16[3,128,512]{2,1,0:T(8,128)(2,1)} %copy-done.13) | copy-start | bytes 1179652
  588.9 29.4 %copy-start.12 = (bf16[3,128,512]{2,1,0:T(8,128)(2,1)S(1)}, bf16[3,128,512]{2,1,0:T(8,128)(2,1)}, u32[]{:S(2)}) copy-start(bf16[3,128,512]{2,1,0:T(8,128)(2,1)} %copy-done.11) | copy-start | bytes 1179652
  588.9 29.5 %copy-start.10 = (bf16[3,128,512]{2,1,0:T(8,128)(2,1)S(1)}, bf16[3,128,512]{2,1,0:T(8,128)(2,1)}, u32[]{:S(2)}) copy-start(bf16[3,128,512]{2,1,0:T(8,128)(2,1)} %copy-done.9) | copy-start | bytes 1179652
  588.9 29.5 %copy-start.8 = (bf16[3,128,512]{2,1,0:T(8,128)(2,1)S(1)}, bf16[3,128,512]{2,1,0:T(8,128)(2,1)}, u32[]{:S(2)}) copy-start(bf16[3,128,512]{2,1,0:T(8,128)(2,1)} %copy-done.7) | copy-start | bytes 1179652
  588.9 29.5 %copy-start.6 = (bf16[3,128,512]{2,1,0:T(8,128)(2,1)S(1)}, bf16[3,128,512]{2,1,0:T(8,128)(2,1)}, u32[]{:S(2)}) copy-start(bf16[3,128,512]{2,1,0:T(8,128)(2,1)} %copy-done.5) | copy-start | bytes 1179652
  588.9 29.6 %copy-start.4 = (bf16[3,128,512]{2,1,0:T(8,128)(2,1)S(1)}, bf16[3,128,512]{2,1,0:T(8,128)(2,1)}, u32[]{:S(2)}) copy-start(bf16[3,128,512]{2,1,0:T(8,128)(2,1)} %copy-done.3) | copy-start | bytes 1179652
  588.9 29.6 %copy-start.2 = (bf16[3,128,512]{2,1,0:T(8,128)(2,1)S(1)}, bf16[3,128,512]{2,1,0:T(8,128)(2,1)}, u32[]{:S(2)}) copy-start(bf16[3,128,512]{2,1,0:T(8,128)(2,1)} %copy-done.1) | copy-start | bytes 1179652
  (13 other events, 9.8 us)
Sparse Core Ops, SparseCore 0:
  18.9 205.4 reduce-scatter.1
  227.7 114.4 all-gather.1
